TPU v7x, 32 devices: a whole 2x2x4 slice. The times are simulated.
32 devices in a mesh: grp: 2 (over y), sp: 4 (over z), fs: 2 (over x), tp: 2 (over core).
Axes of the slice: x: 2, y: 2, z: 4, core: 2. Of those that a mesh axis runs over, the one named last changes fastest.
Arguments:
- tokens: bfloat16 [2, 6144, 2048], P('fs', ('grp', 'sp'), 'tp'), parts along dimension 1, may hold values from -12 to 12
- norm_gain: float32 [2048], replicated, may hold values from 0.1 to 1.9
- query_weight: bfloat16 [2048, 16, 64], P(None, 'tp'), may hold values from -3 to 3
- key_weight: bfloat16 [2048, 4, 64], P(None, 'tp'), may hold values from -3 to 3
- value_weight: bfloat16 [2048, 4, 64], P(None, 'tp'), may hold values from -0.125 to 0.125
- sink_logit: float32 [16], P('tp'), may hold values from 1 to 6
- pool_weight: bfloat16 [2048, 4, 256], P(None, None, 'tp'), may hold values from -0.125 to 0.125
- attn_out_weight: bfloat16 [16, 64, 2048], P('tp'), may hold values from -0.5 to 0.5
- pool_out_weight: bfloat16 [4, 256, 2048], P(None, 'tp'), may hold values from -0.1875 to 0.1875
Outputs:
- mixed: bfloat16 [2, 6144, 2048], P('fs', ('grp', 'sp', 'tp')), parts along dimension 1
There are 2 independent parts, one for each index of `grp`. A program takes and returns all parts, laid end to end along the dimension named above; an argument that names none is the same for every part. Nothing has to cross between parts.
All inputs are finite; a program needn't handle non-finite values.
Results may differ from a plain program's by a relative error of at most 0.0095.
The roundings to bfloat16 on the way count: a program that leaves them out, or rounds other values in their place, can miss the bound.
Values may be sent and summed in bfloat16 or wider, within the bound.
No kernel may reach another device: no remote copies, remote signals or barrier semaphores. Data moves between devices by JAX's collectives and lax.ppermute only.
A program may use at most 128 MiB of HBM per device.

v0:
```python
import jax
import jax.numpy as jnp
from jax import lax
from jax.sharding import PartitionSpec as P

WINDOW = 128


def from_behind(value, axis, steps):
    count = lax.axis_size(axis)
    first, last = (max(0, -steps), min(count, count - steps))
    return lax.ppermute(value, axis, [(source, source + steps) for source in range(first, last)])


def rms_norm(rows, gain):
    values = rows.astype(jnp.float32)
    scale = lax.rsqrt(jnp.mean(values * values, axis=-1, keepdims=True) + 1e-06)
    return (values * scale * gain).astype(jnp.bfloat16)


def attend(query, key, value, key_tail, value_tail, sinks, offset):
    rows = query.shape[0]
    local_kv = key_tail.shape[1]
    head_dim = key_tail.shape[2]
    group = query.shape[1] // (local_kv * head_dim)
    blocks = rows // WINDOW
    qb = query.reshape(blocks, WINDOW, local_kv, group, head_dim)

    def banded(tensor, tail):
        tb = tensor.reshape(blocks, WINDOW, local_kv, head_dim)
        whole = jnp.concatenate([tail, tensor.reshape(rows, local_kv, head_dim)], axis=0)
        before = whole[:rows].reshape(blocks, WINDOW, local_kv, head_dim)
        return jnp.concatenate([before, tb], axis=1)

    kw = banded(key, key_tail)
    vw = banded(value, value_tail)
    qi = jnp.arange(WINDOW, dtype=jnp.int32)[:, None]
    kj = jnp.arange(2 * WINDOW, dtype=jnp.int32)[None, :]
    dist = WINDOW + qi - kj
    inside = (dist >= 0) & (dist < WINDOW)
    key_pos = (
        offset + jnp.arange(blocks, dtype=jnp.int32)[:, None, None] * WINDOW - WINDOW + kj[None]
    )
    mask = inside[None] & (key_pos >= 0)
    scores = jnp.einsum(
        "nqhgd,nkhd->nhgqk", qb, kw, preferred_element_type=jnp.float32
    ) * head_dim ** (-0.5)
    scores = jnp.where(mask[:, None, None], scores, -jnp.inf)
    sink = sinks.reshape(1, local_kv, group, 1, 1)
    top = jnp.maximum(jnp.max(scores, axis=-1, keepdims=True), sink)
    expo = jnp.exp(scores - top)
    total = jnp.sum(expo, axis=-1, keepdims=True) + jnp.exp(sink - top)
    weight = (expo / total).astype(jnp.bfloat16)
    out = jnp.einsum("nhgqk,nkhd->nqhgd", weight, vw, preferred_element_type=jnp.float32)
    return out.reshape(rows, -1).astype(jnp.bfloat16)


def shards(
    tokens,
    norm_gain,
    query_weight,
    key_weight,
    value_weight,
    sink_logit,
    pool_weight,
    attn_out_weight,
    pool_out_weight,
):
    whole = lax.all_gather(tokens, "tp", axis=2, tiled=True)[0]
    rows = whole.shape[0]
    width = whole.shape[1]
    local_kv = key_weight.shape[1]
    head_dim = key_weight.shape[2]
    channels = pool_weight.shape[2]
    normed = rms_norm(whole, norm_gain)
    query = jnp.dot(
        normed, query_weight.reshape(width, -1), preferred_element_type=jnp.float32
    ).astype(jnp.bfloat16)
    key = jnp.dot(normed, key_weight.reshape(width, -1), preferred_element_type=jnp.float32).astype(
        jnp.bfloat16
    )
    value = jnp.dot(
        normed, value_weight.reshape(width, -1), preferred_element_type=jnp.float32
    ).astype(jnp.bfloat16)
    pooled_in = jnp.dot(
        normed, pool_weight.reshape(width, -1), preferred_element_type=jnp.float32
    ).astype(jnp.bfloat16)
    pool_rows = pooled_in.reshape(rows, 4, channels)
    key_rows = key.reshape(rows, local_kv, head_dim)
    value_rows = value.reshape(rows, local_kv, head_dim)
    key_tail, value_tail, pool_tail = from_behind(
        (key_rows[rows - WINDOW :], value_rows[rows - WINDOW :], pool_rows[rows - WINDOW :]),
        "sp",
        1,
    )
    offset = lax.axis_index("sp") * rows
    attended = attend(query, key, value, key_tail, value_tail, sink_logit, offset)
    prefix_total = jnp.sum(pool_rows[:, 3].astype(jnp.float32), axis=0)
    totals = lax.all_gather(prefix_total[None], "sp", axis=0, tiled=True)
    below = jnp.arange(totals.shape[0], dtype=jnp.int32) < lax.axis_index("sp")
    carried = jnp.sum(jnp.where(below[:, None], totals, 0.0), axis=0)
    reaches = jnp.array([2.0, 4.0, 16.0, 1000000000.0], jnp.float32)
    ext = jnp.concatenate([pool_tail, pool_rows], axis=0)
    position = jnp.arange(rows, dtype=jnp.int32)[:, None]
    source = jnp.arange(rows + WINDOW, dtype=jnp.int32)[None, :]
    gap = (position + WINDOW - source).astype(jnp.float32)
    group_ids = jnp.arange(4, dtype=jnp.int32)[:, None, None]
    band = (
        (gap[None] >= 0.0)
        & (gap[None] < reaches[:, None, None])
        & ((group_ids < 3) | (source[None] >= WINDOW))
    )
    sums = jnp.einsum(
        "gij,jgc->igc", band.astype(jnp.bfloat16), ext, preferred_element_type=jnp.float32
    )
    carry_rows = jnp.concatenate([jnp.zeros((3, channels), jnp.float32), carried[None]], axis=0)
    sums = sums + carry_rows[None]
    count = (offset + jnp.arange(1, rows + 1, dtype=jnp.int32)).astype(jnp.float32)
    denom = jnp.minimum(count[:, None], reaches[None, :])[:, :, None]
    pooled = (
        (sums / denom - pool_rows.astype(jnp.float32))
        .astype(jnp.bfloat16)
        .reshape(rows, 4 * channels)
    )
    attn_rows = attn_out_weight.reshape(-1, width)
    pool_weight_rows = pool_out_weight.reshape(-1, width)
    part_sum = jnp.dot(attended, attn_rows, preferred_element_type=jnp.float32)
    result = lax.psum_scatter(
        (part_sum + jnp.dot(pooled, pool_weight_rows, preferred_element_type=jnp.float32)).astype(
            jnp.bfloat16
        ),
        "tp",
        scatter_dimension=0,
        tiled=True,
    )
    return result[None]


def solution(mesh):
    in_specs = (
        P("fs", ("grp", "sp"), "tp"),
        P(),
        P(None, "tp", None),
        P(None, "tp", None),
        P(None, "tp", None),
        P("tp"),
        P(None, None, "tp"),
        P("tp", None, None),
        P(None, "tp", None),
    )
    out_specs = P("fs", ("grp", "sp", "tp"), None)
    return jax.shard_map(shards, mesh=mesh, in_specs=in_specs, out_specs=out_specs, check_vma=False)
```

profile of v0, /device:TPU:0, one launch (start us, length us, event | category | flops | bytes accessed | tf_op | source)
XLA Modules:
  0.0 103.8 jit_solution(3450044622372322319)
XLA Ops:
  6.5 0.7 all-gather.4.cloned.1.call-update
  7.3 0.7 max.18
  8.2 0.7 broadcast_or_fusion
  8.8 0.7 broadcast_minimum_fusion
  9.6 0.3 broadcast_and_fusion
  9.9 1.5 %broadcast_compare_fusion = pred[768,896]{1,0:T(8,128)(4,1)} fusion(s32[768]{0:T(1024)S(1)} %iota_add_fusion), kind=kLoop, calls=%fused_computation.34 | loop fusion | flops 2064384 | bytes 691200 | tf_op jit(solution)/shard_map/ge | solution.py:109
  11.4 1.8 %subtract_convert_fusion = f32[768,896]{1,0:T(8,128)} fusion(s32[768]{0:T(1024)S(1)} %iota_add_fusion), kind=kLoop, calls=%fused_computation.22 | loop fusion | flops 1376256 | bytes 2755584 | tf_op jit(solution)/shard_map/convert_element_type | solution.py:106
  13.1 10.6 %all-gather.4.cloned.1.call-done = bf16[1,768,2048]{2,1,0:T(8,128)(2,1)} async-done(((bf16[1,768,1024]{2,1,0:T(8,128)(2,1)}), bf16[1,768,2048]{2,1,0:T(8,128)(2,1)}) %all-gather.4.cloned.1.call-update) | async-done | bytes 3145744 | tf_op jit(solution)/shard_map/all_gather | solution.py:69
  23.8 2.7 %fusion.4 = f32[768]{0:T(1024)S(1)} fusion(bf16[1,768,2048]{2,1,0:T(8,128)(2,1)} %all-gather.4.cloned.1.call-done), kind=kLoop, calls=%fused_computation.6 | loop fusion | flops 4717824 | bytes 3148800 | tf_op jit(solution)/shard_map/reduce_sum | solution.py:17
  26.6 2.3 %convolution_convert_fusion.2 = bf16[768,128]{0,1:T(8,128)(2,1)S(1)} fusion(bf16[2048,128]{0,1:T(8,128)(2,1)} %bitcast.105, bf16[1,768,2048]{2,1,0:T(8,128)(2,1)S(1)} %copy-done.1, f32[2048]{0:T(1024)S(1)} %copy-done.10, f32[768]{0:T(1024)S(1)} %add_rsqrt_fusion), kind=kOutput, calls=%fused_computation.37 | convolution fusion | flops 409042944 | bytes 3877888 | tf_op jit(solution)/shard_map/dot_general | solution.py:82
  28.9 0.2 reshape.317
  29.2 3.4 %convolution_convert_fusion.1 = bf16[768,128]{0,1:T(8,128)(2,1)S(1)} fusion(bf16[2048,128]{0,1:T(8,128)(2,1)} %bitcast.106, bf16[1,768,2048]{2,1,0:T(8,128)(2,1)} %all-gather.4.cloned.1.call-done, f32[2048]{0:T(1024)S(1)} %copy-done.10, f32[768]{0:T(1024)S(1)} %add_rsqrt_fusion), kind=kOutput, calls=%fused_computation.36 | convolution fusion | flops 409042944 | bytes 3877888 | tf_op jit(solution)/shard_map/dot_general | solution.py:79
  32.6 4.3 %collective-permute-start.1 = (bf16[128,2,64]{0,2,1:T(8,128)(2,1)S(1)}, bf16[128,2,64]{0,2,1:T(8,128)(2,1)}, u32[]{:S(2)}, u32[]{:S(2)}) collective-permute-start(bf16[128,2,64]{0,2,1:T(8,128)(2,1)S(1)} %bitcast.99), channel_id=1, source_target_pairs={{0,4},{4,8},{8,12},{1,5},{5,9},{9,13},{2,6},{6,10},{10,14},{3,7},{... | collective-permute-start | bytes 98312 | tf_op jit(solution)/shard_map/ppermute | solution.py:12
  36.9 3.4 %collective-permute-start = (bf16[128,2,64]{0,2,1:T(8,128)(2,1)S(1)}, bf16[128,2,64]{0,2,1:T(8,128)(2,1)}, u32[]{:S(2)}, u32[]{:S(2)}) collective-permute-start(bf16[128,2,64]{0,2,1:T(8,128)(2,1)S(1)} %bitcast.98), channel_id=1, source_target_pairs={{0,4},{4,8},{8,12},{1,5},{5,9},{9,13},{2,6},{6,10},{10,14},{3,7},{... | collective-permute-start | bytes 98312 | tf_op jit(solution)/shard_map/ppermute | solution.py:12
  40.3 2.0 %fusion.25 = bf16[768,512]{0,1:T(8,128)(2,1)S(1)} fusion(bf16[256,8,4,128]{3,2,1,0:T(4,128)(2,1)S(1)} %bitcast.103, bf16[1,768,2048]{2,1,0:T(8,128)(2,1)S(1)} %copy-done.2, f32[2048]{0:T(1024)S(1)} %copy-done.10, f32[768]{0:T(1024)S(1)} %add_rsqrt_fusion), kind=kOutput, calls=%fused_computation.31 | convolution fusion | flops 1617297408 | bytes 6040576 | tf_op jit(solution)/shard_map/dot_general | solution.py:85
  42.4 0.1 convert_reduce_fusion
  42.5 8.5 %all-gather.1 = f32[4,1,128]{2,1,0:T(1,128)S(1)} all-gather(f32[1,1,128]{2,1,0:T(1,128)S(1)} %bitcast.101), channel_id=2, replica_groups=mesh['grp'=2,'sp'=4,'fs'=2,'tp'=2] {'sp'}, dimensions={0}, use_global_device_ids=true | all-gather | bytes 2560 | tf_op jit(solution)/shard_map/all_gather | solution.py:99
  50.9 3.7 %collective-permute-start.2 = (bf16[128,4,128]{0,2,1:T(8,128)(2,1)S(1)}, bf16[128,4,128]{0,2,1:T(8,128)(2,1)}, u32[]{:S(2)}, u32[]{:S(2)}) collective-permute-start(bf16[128,4,128]{0,2,1:T(8,128)(2,1)S(1)} %bitcast.97), channel_id=1, source_target_pairs={{0,4},{4,8},{8,12},{1,5},{5,9},{9,13},{2,6},{6,10},{10,14},{3,7},{... | collective-permute-start | bytes 393224 | tf_op jit(solution)/shard_map/ppermute | solution.py:12
  54.6 2.7 %convolution_convert_fusion = bf16[768,512]{1,0:T(8,128)(2,1)} fusion(bf16[2048,512]{0,1:T(8,128)(2,1)S(1)} %bitcast.104, bf16[1,768,2048]{2,1,0:T(8,128)(2,1)S(1)} %copy-done.2, f32[2048]{0:T(1024)S(1)} %copy-done.10, f32[768]{0:T(1024)S(1)} %add_rsqrt_fusion), kind=kOutput, calls=%fused_computation.32 | convolution fusion | flops 1617297408 | bytes 6040576 | tf_op jit(solution)/shard_map/dot_general | solution.py:76
  57.4 0.7 select_reduce_fusion
  58.0 0.2 reshape.321
  58.3 3.6 %reshape.334 = bf16[6,128,2,4,64]{4,3,2,1,0:T(4,128)(2,1)} reshape(bf16[768,512]{1,0:T(8,128)(2,1)} %convolution_convert_fusion) | data formatting | bytes 1572864 | tf_op jit(solution)/shard_map/reshape | solution.py:27
  61.9 1.3 %concatenate.23 = f32[4,128]{1,0:T(4,128)} pad(f32[1,128]{1,0:T(1,128)} %bitcast.102, f32[]{:T(128)} %constant.14.clone.1), padding=3_0x0_0 | pad | bytes 2564 | tf_op jit(solution)/shard_map/concatenate | solution.py:116
  63.2 0.8 copy_bitcast_fusion
  64.0 2.7 %fusion.13 = (f32[6,2,4,128]{3,2,1,0:T(4,128)S(1)}, f32[6,2,256,128,4]{3,2,4,1,0:T(8,128)S(1)}) fusion(pred[6,128,256]{1,2,0:T(8,128)(4,1)S(1)} %broadcast_and_fusion, bf16[6,128,2,4,64]{4,3,2,1,0:T(4,128)(2,1)} %reshape.334, bf16[6,128,2,64]{1,3,2,0:T(8,128)(2,1)S(1)} %copy.28, bf16[6,128,2,64]{1,3,2,0:T(8,128)(2,1)S(1)} %copy_bitcast_fusion), kind=kOutput, calls=%fused_computation.19 | convolution fusion | flops 206825472 | bytes 7692288 | tf_op jit(solution)/shard_map/nqhgd,nkhd->nhgqk/dot_general | solution.py:45
  66.8 1.7 %fusion.8 = f32[6,2,4,128]{3,2,1,0:T(4,128)S(1)} fusion(f32[6,2,256,128,4]{3,2,4,1,0:T(8,128)S(1)} %get-tuple-element.6, f32[6,2,4,128]{3,2,1,0:T(4,128)S(1)} %broadcast_maximum_fusion, pred[6,128,256]{1,2,0:T(8,128)(4,1)S(1)} %broadcast_and_fusion), kind=kLoop, calls=%fused_computation.14 | loop fusion | flops 6285312 | bytes 6537216 | tf_op jit(solution)/shard_map/reduce_sum | solution.py:52
  68.5 0.8 copy_bitcast_fusion.1
  69.3 1.7 %fusion.31 = bf16[6,128,2,4,64]{1,4,3,2,0:T(8,128)(2,1)S(1)} fusion(f32[6,2,256,128,4]{3,2,4,1,0:T(8,128)S(1)} %get-tuple-element.6, f32[6,2,4,128]{3,2,1,0:T(4,128)S(1)} %exponential_add_fusion, f32[6,2,4,128]{3,2,1,0:T(4,128)S(1)} %broadcast_maximum_fusion, pred[6,128,256]{1,2,0:T(8,128)(4,1)S(1)} %broadcast_and_fusion, ...), kind=kOutput, calls=%fused_computation.35 | convolution fusion | flops 210370560 | bytes 7716864 | tf_op jit(solution)/shard_map/nhgqk,nkhd->nqhgd/dot_general | solution.py:54
  71.1 0.6 copy.32
  71.7 4.5 %fusion.38 = f32[768,2048]{1,0:T(8,128)} fusion(bf16[512,2048]{1,0:T(8,128)(2,1)S(1)} %bitcast.91, bf16[64,8,6,128]{3,2,1,0:T(8,128)(2,1)S(1)} %bitcast.92), kind=kOutput, calls=%fused_computation.41 | convolution fusion | flops 1610612736 | bytes 9175040 | tf_op jit(solution)/shard_map/dot_general | solution.py:127
  76.2 11.3 %fusion.7 = bf16[768,2048]{1,0:T(8,128)(2,1)} fusion(f32[768,2048]{1,0:T(8,128)} %fusion.38, bf16[4,128,2048]{2,1,0:T(8,128)(2,1)} %param.18, bf16[768,4,128]{0,2,1:T(8,128)(2,1)} %bitcast.96, f32[768,896]{1,0:T(8,128)} %subtract_convert_fusion, f32[4]{0:T(128)S(1)} %copy-done.7, pred[4,896]{1,0:T(4,128)(4,1)S(1)} %copy-done.5, ...), kind=kOutput, calls=%fused_computation.10 | convolution fusion | flops 2330460160 | bytes 15910416 | tf_op jit(solution)/shard_map/dot_general | solution.py:129
  87.5 9.5 %reduce-scatter.2.cloned.1.call-done = bf16[384,2048]{1,0:T(8,128)(2,1)} async-done(((bf16[768,2048]{1,0:T(8,128)(2,1)}), bf16[384,2048]{1,0:T(8,128)(2,1)}) %reduce-scatter.2.cloned.1.call-update) | async-done | bytes 1572880 | tf_op jit(solution)/shard_map/reduce_scatter | solution.py:128
  (45 shorter events, 0.6 us)
Async XLA Ops:
  6.5 65.1 %copy-start = (bf16[8,64,2048]{2,1,0:T(8,128)(2,1)S(1)}, bf16[8,64,2048]{2,1,0:T(8,128)(2,1)}, u32[]{:S(2)}) copy-start(bf16[8,64,2048]{2,1,0:T(8,128)(2,1)} %param.17) | copy-start | bytes 6291460
  6.5 17.2 %all-gather.4.cloned.1.call-start = ((), (), s32[]{:S(2)}) async-start(), calls=%async_computation.1 | async-start | bytes 4718592 | tf_op jit(solution)/shard_map/all_gather | solution.py:69
  7.3 89.7 %reduce-scatter.2.cloned.1.call-start = ((), (), s32[]{:S(2)}) async-start(), calls=%async_computation.2 | async-start | bytes 4718592 | tf_op jit(solution)/shard_map/reduce_scatter | solution.py:128
  9.9 16.6 %copy-start.10 = (f32[2048]{0:T(1024)S(1)}, f32[2048]{0:T(1024)}, u32[]{:S(2)}) copy-start(f32[2048]{0:T(1024)} %param.11) | copy-start | bytes 24580
  23.8 2.8 %copy-start.1 = (bf16[1,768,2048]{2,1,0:T(8,128)(2,1)S(1)}, bf16[1,768,2048]{2,1,0:T(8,128)(2,1)}, u32[]{:S(2)}) copy-start(bf16[1,768,2048]{2,1,0:T(8,128)(2,1)} %all-gather.4.cloned.1.call-done) | copy-start | bytes 9437188
  29.2 11.1 %copy-start.2 = (bf16[1,768,2048]{2,1,0:T(8,128)(2,1)S(1)}, bf16[1,768,2048]{2,1,0:T(8,128)(2,1)}, u32[]{:S(2)}) copy-start(bf16[1,768,2048]{2,1,0:T(8,128)(2,1)} %all-gather.4.cloned.1.call-done) | copy-start | bytes 9437188
  29.2 11.1 %copy-start.8 = (bf16[2048,4,128]{2,1,0:T(4,128)(2,1)S(1)}, bf16[2048,4,128]{2,1,0:T(4,128)(2,1)}, u32[]{:S(2)}) copy-start(bf16[2048,4,128]{2,1,0:T(4,128)(2,1)} %param.16) | copy-start | bytes 6291460
  32.6 30.6 %collective-permute-start.1 = (bf16[128,2,64]{0,2,1:T(8,128)(2,1)S(1)}, bf16[128,2,64]{0,2,1:T(8,128)(2,1)}, u32[]{:S(2)}, u32[]{:S(2)}) collective-permute-start(bf16[128,2,64]{0,2,1:T(8,128)(2,1)S(1)} %bitcast.99), channel_id=1, source_target_pairs={{0,4},{4,8},{8,12},{1,5},{5,9},{9,13},{2,6},{6,10},{10,14},{3,7},{... | collective-permute-start | bytes 98312 | tf_op jit(solution)/shard_map/ppermute | solution.py:12
  36.9 31.7 %collective-permute-start = (bf16[128,2,64]{0,2,1:T(8,128)(2,1)S(1)}, bf16[128,2,64]{0,2,1:T(8,128)(2,1)}, u32[]{:S(2)}, u32[]{:S(2)}) collective-permute-start(bf16[128,2,64]{0,2,1:T(8,128)(2,1)S(1)} %bitcast.98), channel_id=1, source_target_pairs={{0,4},{4,8},{8,12},{1,5},{5,9},{9,13},{2,6},{6,10},{10,14},{3,7},{... | collective-permute-start | bytes 98312 | tf_op jit(solution)/shard_map/ppermute | solution.py:12
  40.3 14.3 %copy-start.9 = (bf16[2048,8,64]{0,2,1:T(8,128)(2,1)S(1)}, bf16[2048,8,64]{0,2,1:T(8,128)(2,1)}, u32[]{:S(2)}) copy-start(bf16[2048,8,64]{0,2,1:T(8,128)(2,1)} %param.12) | copy-start | bytes 6291460
  42.3 15.0 %copy-start.4 = (bf16[768,512]{0,1:T(8,128)(2,1)}, bf16[768,512]{0,1:T(8,128)(2,1)S(1)}, u32[]{:S(2)}) copy-start(bf16[768,512]{0,1:T(8,128)(2,1)S(1)} %fusion.25) | copy-start | bytes 2359300
  50.9 25.2 %collective-permute-start.2 = (bf16[128,4,128]{0,2,1:T(8,128)(2,1)S(1)}, bf16[128,4,128]{0,2,1:T(8,128)(2,1)}, u32[]{:S(2)}, u32[]{:S(2)}) collective-permute-start(bf16[128,4,128]{0,2,1:T(8,128)(2,1)S(1)} %bitcast.97), channel_id=1, source_target_pairs={{0,4},{4,8},{8,12},{1,5},{5,9},{9,13},{2,6},{6,10},{10,14},{3,7},{... | collective-permute-start | bytes 393224 | tf_op jit(solution)/shard_map/ppermute | solution.py:12
  71.6 4.5 %copy-start.3 = (pred[768,896]{1,0:T(8,128)(4,1)S(1)}, pred[768,896]{1,0:T(8,128)(4,1)}, u32[]{:S(2)}) copy-start(pred[768,896]{1,0:T(8,128)(4,1)} %broadcast_compare_fusion) | copy-start | bytes 2064388
  71.7 4.5 %copy-start.5 = (pred[4,896]{1,0:T(4,128)(4,1)S(1)}, pred[4,896]{1,0:T(4,128)(4,1)}, u32[]{:S(2)}) copy-start(pred[4,896]{1,0:T(4,128)(4,1)} %broadcast_or_fusion) | copy-start | bytes 10756
  71.7 4.5 %copy-start.6 = (f32[4,128]{1,0:T(4,128)S(1)}, f32[4,128]{1,0:T(4,128)}, u32[]{:S(2)}) copy-start(f32[4,128]{1,0:T(4,128)} %concatenate.23) | copy-start | bytes 6148
  71.7 4.5 %copy-start.7 = (f32[4]{0:T(128)S(1)}, f32[4]{0:T(128)}, u32[]{:S(2)}) copy-start(f32[4]{0:T(128)} %constant.13.clone) | copy-start | bytes 52
Sparse Core Ops, SparseCore 0:
  8.9 14.8 all-gather.3
  87.7 9.2 reduce-scatter.1
where the time goes:
time: 104 us
  matrix products  30.6 us (29%)
  waiting for transfers between devices  20.8 us (20%)
  between operations  13.7 us (13%)
  other arithmetic  12 us (12%)
  starting transfers between devices  11.4 us (11%)
  blocking collectives  8.46 us (8%)
  local copies, waits for them, and re-layouts  6.9 us (7%)
    ppermute x3, starting transfers between devices, from_behind(): lax.ppermute(value, axis, [(source, source + steps) for source in range(f...  11.3 us
    dot_general x1, matrix products, shards(): jnp.dot(pooled, pool_weight_rows, preferred_element_type=jnp.float32)  11.3 us
    all_gather x1, waiting for transfers between devices, shards(): whole = lax.all_gather(tokens, 'tp', axis=2, tiled=True)[0]  10.6 us
    reduce_scatter x1, waiting for transfers between devices, shards(): lax.psum_scatter((part_sum + jnp.dot(pooled, pool_weight_rows, preferred_...  9.46 us
    all_gather x1, blocking collectives, shards(): totals = lax.all_gather(prefix_total[None], 'sp', axis=0, tiled=True)  8.46 us
    dot_general x1, matrix products, shards(): part_sum = jnp.dot(attended, attn_rows, preferred_element_type=jnp.float32)  4.48 us
    reshape x1, local copies, waits for them, and re-layouts, attend(): qb = query.reshape(blocks, WINDOW, local_kv, group, head_dim)  3.63 us
    dot_general x1, matrix products, shards(): jnp.dot(normed, key_weight.reshape(width, -1), preferred_element_type=jnp...  3.38 us
  transfers between devices with their start and end apart: 5, of which 2 were waited for; matrix products, arithmetic and copies ran while one was open for 28% of the time, Pallas kernels for 0%

commit v1 on v0

--- a/solution.py
+++ b/solution.py
@@ -8,8 +8,11 @@
 
 def from_behind(value, axis, steps):
     count = lax.axis_size(axis)
-    first, last = (max(0, -steps), min(count, count - steps))
-    return lax.ppermute(value, axis, [(source, source + steps) for source in range(first, last)])
+    return lax.ppermute(value, axis, [(i, (i + steps) % count) for i in range(count)])
+
+
+def swap(value):
+    return lax.ppermute(value, "tp", [(0, 1), (1, 0)])
 
 
 def rms_norm(rows, gain):
@@ -66,7 +69,12 @@
     attn_out_weight,
     pool_out_weight,
 ):
-    whole = lax.all_gather(tokens, "tp", axis=2, tiled=True)[0]
+    mine = tokens[0]
+    other = swap(mine)
+    side = lax.axis_index("tp")
+    whole = jnp.concatenate(
+        [jnp.where(side == 0, mine, other), jnp.where(side == 0, other, mine)], axis=1
+    )
     rows = whole.shape[0]
     width = whole.shape[1]
     local_kv = key_weight.shape[1]
@@ -88,17 +96,26 @@
     pool_rows = pooled_in.reshape(rows, 4, channels)
     key_rows = key.reshape(rows, local_kv, head_dim)
     value_rows = value.reshape(rows, local_kv, head_dim)
-    key_tail, value_tail, pool_tail = from_behind(
-        (key_rows[rows - WINDOW :], value_rows[rows - WINDOW :], pool_rows[rows - WINDOW :]),
-        "sp",
-        1,
+    place = lax.axis_index("sp")
+    tails = jnp.concatenate(
+        [key[rows - WINDOW :], value[rows - WINDOW :], pooled_in[rows - WINDOW :]], axis=1
     )
+    tails = jnp.where(place > 0, from_behind(tails, "sp", 1), 0)
+    narrow = local_kv * head_dim
+    key_tail = tails[:, :narrow].reshape(WINDOW, local_kv, head_dim)
+    value_tail = tails[:, narrow : 2 * narrow].reshape(WINDOW, local_kv, head_dim)
+    pool_tail = tails[:, 2 * narrow :].reshape(WINDOW, 4, channels)
     offset = lax.axis_index("sp") * rows
     attended = attend(query, key, value, key_tail, value_tail, sink_logit, offset)
     prefix_total = jnp.sum(pool_rows[:, 3].astype(jnp.float32), axis=0)
-    totals = lax.all_gather(prefix_total[None], "sp", axis=0, tiled=True)
-    below = jnp.arange(totals.shape[0], dtype=jnp.int32) < lax.axis_index("sp")
-    carried = jnp.sum(jnp.where(below[:, None], totals, 0.0), axis=0)
+    running = prefix_total
+    carried = jnp.zeros_like(prefix_total)
+    step = 1
+    while step < lax.axis_size("sp"):
+        got = jnp.where(place >= step, from_behind(running, "sp", step), 0.0)
+        carried = carried + got
+        running = running + got
+        step *= 2
     reaches = jnp.array([2.0, 4.0, 16.0, 1000000000.0], jnp.float32)
     ext = jnp.concatenate([pool_tail, pool_rows], axis=0)
     position = jnp.arange(rows, dtype=jnp.int32)[:, None]
@@ -124,15 +141,22 @@
     )
     attn_rows = attn_out_weight.reshape(-1, width)
     pool_weight_rows = pool_out_weight.reshape(-1, width)
-    part_sum = jnp.dot(attended, attn_rows, preferred_element_type=jnp.float32)
-    result = lax.psum_scatter(
-        (part_sum + jnp.dot(pooled, pool_weight_rows, preferred_element_type=jnp.float32)).astype(
-            jnp.bfloat16
-        ),
-        "tp",
-        scatter_dimension=0,
-        tiled=True,
-    )
+    half = rows // 2
+
+    def project(start):
+        part = jnp.dot(
+            lax.dynamic_slice_in_dim(attended, start, half, 0),
+            attn_rows,
+            preferred_element_type=jnp.float32,
+        )
+        return part + jnp.dot(
+            lax.dynamic_slice_in_dim(pooled, start, half, 0),
+            pool_weight_rows,
+            preferred_element_type=jnp.float32,
+        )
+
+    given = swap(project((1 - side) * half).astype(jnp.bfloat16))
+    result = (project(side * half) + given.astype(jnp.float32)).astype(jnp.bfloat16)
     return result[None]
 
 

time: 104 us -> 52.6 us (0.51)
  waiting for transfers between devices: 20.8 us -> 2.74 us
  between operations: 13.7 us -> 0.39 us
  blocking collectives: 8.46 us -> 0 us
  matrix products: 30.6 us -> 25.1 us
  starting transfers between devices: 11.4 us -> 5.94 us
  other arithmetic: 12 us -> 10.7 us
    all_gather x1 -> x0, waiting for transfers between devices: 10.6 us -> none  [shards(): whole = lax.all_gather(tokens, 'tp', axis=2, tiled=True)[0]]
    reduce_scatter x1 -> x0, waiting for transfers between devices: 9.46 us -> none  [shards(): lax.psum_scatter((part_sum + jnp.dot(pooled, pool_weight_rows, preferred_...]
    all_gather x1 -> x0, blocking collectives: 8.46 us -> none  [shards(): totals = lax.all_gather(prefix_total[None], 'sp', axis=0, tiled=True)]
    ppermute x3 -> x5, starting transfers between devices: 11.3 us -> 5.94 us  [the longest x3 5.45 us: from_behind(): lax.ppermute(value, axis, [(i, (i + steps) % count) for i in range(count)])]
    dot_general x2 -> x5, matrix products: 15.8 us -> 11.3 us  [the longest x2 5.93 us: project(): jnp.dot(lax.dynamic_slice_in_dim(pooled, start, half, 0), pool_weight_row...]
    ppermute x3 -> x5, waiting for transfers between devices: 0.01 us -> 2.74 us  [the longest x2 2.73 us: swap(): return lax.ppermute(value, 'tp', [(0, 1), (1, 0)])]
    dot_general x1, matrix products: 2.72 us -> 5.23 us  [shards(): jnp.dot(normed, query_weight.reshape(width, -1), preferred_element_type=j...]
    dot_general x1, matrix products: 3.38 us -> 1.17 us  [shards(): jnp.dot(normed, key_weight.reshape(width, -1), preferred_element_type=jnp...]
  transfers between devices with their start and end apart: 5 -> 5, of which waited for: 2 -> 1; matrix products, arithmetic and copies ran while one was open for 28% -> 36% of each run, Pallas kernels for 0% -> 0%
where the time goes in v1:
time: 52.6 us; the launch traced here: 52.3 us
  matrix products  25.1 us (48%)
  other arithmetic  10.7 us (20%)
  local copies, waits for them, and re-layouts  7.34 us (14%)
  starting transfers between devices  5.94 us (11%)
  waiting for transfers between devices  2.74 us (5%)
    dot_general x2, matrix products, project(): jnp.dot(lax.dynamic_slice_in_dim(pooled, start, half, 0), pool_weight_row...  5.93 us
    ppermute x3, starting transfers between devices, from_behind(): lax.ppermute(value, axis, [(i, (i + steps) % count) for i in range(count)])  5.45 us
    dot_general x1, matrix products, shards(): jnp.dot(normed, query_weight.reshape(width, -1), preferred_element_type=j...  5.23 us
    reshape x1, local copies, waits for them, and re-layouts, attend(): qb = query.reshape(blocks, WINDOW, local_kv, group, head_dim)  3.63 us
    dot_general x1, matrix products, shards(): jnp.einsum('gij,jgc->igc', band.astype(jnp.bfloat16), ext, preferred_elem...  3.35 us
    ppermute x2, waiting for transfers between devices, swap(): return lax.ppermute(value, 'tp', [(0, 1), (1, 0)])  2.73 us
    dot_general x1, matrix products, attend(): jnp.einsum('nqhgd,nkhd->nhgqk', qb, kw, preferred_element_type=jnp.float32)  2.67 us
    dot_general x2, matrix products, project(): jnp.dot(lax.dynamic_slice_in_dim(attended, start, half, 0), attn_rows, pr...  2.04 us
  transfers between devices with their start and end apart: 5, of which 1 were waited for; matrix products, arithmetic and copies ran while one was open for 36% of the time, Pallas kernels for 0%

profile of v1, /device:TPU:0, one launch (start us, length us, event | category | flops | bytes accessed | tf_op | source)
XLA Modules:
  0.0 52.3 jit_solution(10765854737067831220)
XLA Ops:
  0.0 0.5 collective-permute-start
  0.6 0.8 %max.18 = f32[2,4]{1,0:T(2,128)S(1)} reshape(f32[8]{0:T(128)} %param.15) | data formatting | bytes 64 | tf_op jit(solution)/shard_map/max | solution.py:53
  1.5 0.8 %broadcast_minimum_fusion = f32[768,4]{0,1:T(4,128)S(1)} fusion(f32[4]{0:T(128)} %constant.17.clone, f32[768]{0:T(1024)S(1)} %add_convert_fusion.2), kind=kLoop, calls=%fused_computation.75 | loop fusion | flops 3072 | bytes 15376 | tf_op jit(solution)/shard_map/min | solution.py:136
  2.3 0.3 broadcast_and_fusion
  2.6 1.5 %broadcast_compare_fusion = pred[768,896]{1,0:T(8,128)(4,1)} fusion(s32[768]{0:T(1024)S(1)} %iota_add_fusion), kind=kLoop, calls=%fused_computation.37 | loop fusion | flops 2064384 | bytes 691200 | tf_op jit(solution)/shard_map/ge | solution.py:126
  4.1 1.8 %subtract_convert_fusion = f32[768,896]{1,0:T(8,128)} fusion(s32[768]{0:T(1024)S(1)} %iota_add_fusion), kind=kLoop, calls=%fused_computation.22 | loop fusion | flops 1376256 | bytes 2755584 | tf_op jit(solution)/shard_map/convert_element_type | solution.py:123
  5.9 1.6 %broadcast_select_fusion.1 = (bf16[768,1024]{1,0:T(8,128)(2,1)S(1)}, bf16[768,1024]{1,0:T(8,128)(2,1)S(1)}) fusion(bf16[768,1024]{1,0:T(8,128)(2,1)} %collective-permute-done, pred[]{:T(512)S(6)} %eq.4, bf16[1,768,1024]{2,1,0:T(8,128)(2,1)S(1)} %copy-done.5), kind=kLoop, calls=%fused_computation.33 | loop fusion | flops 1572864 | bytes 6291457 | tf_op jit(solution)/shard_map/jit(_where)/select_n | solution.py:76
  7.5 0.7 %fusion.4 = f32[768]{0:T(1024)S(1)} fusion(bf16[768,1024]{1,0:T(8,128)(2,1)S(1)} %get-tuple-element.6, bf16[768,1024]{1,0:T(8,128)(2,1)S(1)} %get-tuple-element.5), kind=kLoop, calls=%fused_computation.6 | loop fusion | flops 9436416 | bytes 3148800 | tf_op jit(solution)/shard_map/reduce_sum | solution.py:20
  8.2 1.1 %fusion.6 = bf16[768,2048]{1,0:T(8,128)(2,1)S(1)} fusion(f32[2048]{0:T(1024)S(1)} %copy-done.12, f32[768]{0:T(1024)S(1)} %add_rsqrt_fusion, bf16[768,1024]{1,0:T(8,128)(2,1)S(1)} %get-tuple-element.6, bf16[768,1024]{1,0:T(8,128)(2,1)S(1)} %get-tuple-element.5), kind=kLoop, calls=%fused_computation.8 | loop fusion | flops 11010048 | bytes 6302720 | tf_op jit(solution)/shard_map/convert_element_type | solution.py:21
  9.3 0.5 copy-done.14
  9.8 1.8 %fusion.22 = bf16[768,512]{0,1:T(8,128)(2,1)S(1)} fusion(bf16[768,2048]{1,0:T(8,128)(2,1)S(1)} %fusion.6, bf16[256,8,4,128]{3,2,1,0:T(4,128)(2,1)S(1)} %bitcast.107), kind=kOutput, calls=%fused_computation.34 | convolution fusion | flops 1611005952 | bytes 6029312 | tf_op jit(solution)/shard_map/dot_general | solution.py:93
  11.8 2.7 %collective-permute-start.2 = (f32[128]{0:T(128)S(1)}, f32[128]{0:T(128)S(1)}, u32[]{:S(2)}, u32[]{:S(2)}) collective-permute-start(f32[128]{0:T(128)S(1)} %convert_reduce_fusion), channel_id=1, source_target_pairs={{0,4},{4,8},{8,12},{12,0},{1,5},{5,9},{9,13},{13,1},{2,6},{6,10},{... | collective-permute-start | bytes 1544 | tf_op jit(solution)/shard_map/ppermute | solution.py:11
  14.5 1.2 %convolution_convert_fusion.2 = bf16[768,128]{0,1:T(8,128)(2,1)S(1)} fusion(bf16[768,2048]{1,0:T(8,128)(2,1)S(1)} %fusion.6, bf16[2048,128]{0,1:T(8,128)(2,1)S(1)} %bitcast.109), kind=kOutput, calls=%fused_computation.40 | convolution fusion | flops 402751488 | bytes 3866624 | tf_op jit(solution)/shard_map/dot_general | solution.py:87
  15.8 1.2 %convolution_convert_fusion.1 = bf16[768,128]{0,1:T(8,128)(2,1)S(1)} fusion(bf16[768,2048]{1,0:T(8,128)(2,1)S(1)} %fusion.6, bf16[2048,128]{0,1:T(8,128)(2,1)S(1)} %bitcast.110), kind=kOutput, calls=%fused_computation.39 | convolution fusion | flops 402751488 | bytes 3866624 | tf_op jit(solution)/shard_map/dot_general | solution.py:90
  17.0 0.7 %pad_maximum_fusion.3 = bf16[128,768]{0,1:T(8,128)(2,1)} fusion(bf16[128,512]{0,1:T(8,128)(2,1)S(1)} %slice.38, bf16[128,128]{0,1:T(8,128)(2,1)S(1)} %slice.37, bf16[128,128]{0,1:T(8,128)(2,1)S(1)} %slice.36), kind=kLoop, calls=%fused_computation.65 | loop fusion | flops 589824 | bytes 393216 | tf_op jit(solution)/shard_map/concatenate | solution.py:100
  17.6 0.2 reshape.269
  17.9 1.6 %collective-permute-start.1 = (bf16[128,768]{0,1:T(8,128)(2,1)}, bf16[128,768]{0,1:T(8,128)(2,1)}, u32[]{:S(2)}, u32[]{:S(2)}) collective-permute-start(bf16[128,768]{0,1:T(8,128)(2,1)} %pad_maximum_fusion.3), channel_id=1, source_target_pairs={{0,4},{4,8},{8,12},{12,0},{1,5},{5,9},{9,13},{13,1},{2,6},{6,10},{... | collective-permute-start | bytes 589832 | tf_op jit(solution)/shard_map/ppermute | solution.py:11
  19.5 1.1 %collective-permute-start.3 = (f32[128]{0:T(128)S(1)}, f32[128]{0:T(128)S(1)}, u32[]{:S(2)}, u32[]{:S(2)}) collective-permute-start(f32[128]{0:T(128)S(1)} %fusion.55), channel_id=1, source_target_pairs={{0,8},{4,12},{8,0},{12,4},{1,9},{5,13},{9,1},{13,5},{2,10},{6,14},... | collective-permute-start | bytes 1544 | tf_op jit(solution)/shard_map/ppermute | solution.py:11
  20.6 5.2 %convolution_convert_fusion = bf16[768,512]{1,0:T(8,128)(2,1)} fusion(bf16[768,2048]{1,0:T(8,128)(2,1)} %copy-done.3, bf16[2048,512]{0,1:T(8,128)(2,1)} %bitcast.108), kind=kOutput, calls=%fused_computation.35 | convolution fusion | flops 1611005952 | bytes 6029312 | tf_op jit(solution)/shard_map/dot_general | solution.py:84
  26.1 3.6 %reshape.283 = bf16[6,128,2,4,64]{4,3,2,1,0:T(4,128)(2,1)} reshape(bf16[768,512]{1,0:T(8,128)(2,1)} %convolution_convert_fusion) | data formatting | bytes 1572864 | tf_op jit(solution)/shard_map/reshape | solution.py:30
  30.0 2.7 %fusion.12 = (f32[6,2,4,128]{3,2,1,0:T(4,128)S(1)}, f32[6,2,256,128,4]{3,2,4,1,0:T(8,128)S(1)}) fusion(pred[6,128,256]{1,2,0:T(8,128)(4,1)S(1)} %broadcast_and_fusion, bf16[6,128,2,4,64]{4,3,2,1,0:T(4,128)(2,1)} %reshape.283, bf16[6,128,2,64]{1,3,2,0:T(8,128)(2,1)S(1)} %copy.18, bf16[6,128,2,64]{1,3,2,0:T(8,128)(2,1)S(1)} %copy_bitcast_fusion.1), kind=kOutput, calls=%fused_computation.17 | convolution fusion | flops 206825472 | bytes 7692288 | tf_op jit(solution)/shard_map/nqhgd,nkhd->nhgqk/dot_general | solution.py:48
  32.7 1.7 %fusion.7 = f32[6,2,4,128]{3,2,1,0:T(4,128)S(1)} fusion(f32[6,2,256,128,4]{3,2,4,1,0:T(8,128)S(1)} %get-tuple-element.10, f32[6,2,4,128]{3,2,1,0:T(4,128)S(1)} %broadcast_maximum_fusion, pred[6,128,256]{1,2,0:T(8,128)(4,1)S(1)} %broadcast_and_fusion), kind=kLoop, calls=%fused_computation.12 | loop fusion | flops 6285312 | bytes 6537216 | tf_op jit(solution)/shard_map/reduce_sum | solution.py:55
  34.5 1.7 %fusion.26 = bf16[6,128,2,4,64]{1,4,3,2,0:T(8,128)(2,1)S(1)} fusion(f32[6,2,256,128,4]{3,2,4,1,0:T(8,128)S(1)} %get-tuple-element.10, f32[6,2,4,128]{3,2,1,0:T(4,128)S(1)} %exponential_add_fusion, f32[6,2,4,128]{3,2,1,0:T(4,128)S(1)} %broadcast_maximum_fusion, pred[6,128,256]{1,2,0:T(8,128)(4,1)S(1)} %broadcast_and_fusion, ...), kind=kOutput, calls=%fused_computation.38 | convolution fusion | flops 210370560 | bytes 7716864 | tf_op jit(solution)/shard_map/nhgqk,nkhd->nqhgd/dot_general | solution.py:57
  36.3 0.6 %copy.22 = bf16[6,128,2,4,64]{1,0,4,3,2:T(8,128)(2,1)S(1)} copy(bf16[6,128,2,4,64]{1,4,3,2,0:T(8,128)(2,1)S(1)} %fusion.26) | data formatting | bytes 1572864 | tf_op jit(solution)/shard_map/convert_element_type | solution.py:58
  37.0 1.0 %fusion.39 = f32[384,2048]{1,0:T(8,128)S(1)} fusion(bf16[512,2048]{1,0:T(8,128)(2,1)S(1)} %bitcast.91, bf16[768,512]{0,1:T(8,128)(2,1)S(1)} %bitcast.95, s32[]{:T(128)S(6)} %select_n.57), kind=kOutput, calls=%fused_computation.52 | convolution fusion | flops 805306368 | bytes 5636100 | tf_op jit(solution)/shard_map/dot_general | solution.py:147
  38.1 0.7 %copy-done.4 = f32[768,896]{1,0:T(8,128)S(1)} copy-done((f32[768,896]{1,0:T(8,128)S(1)}, f32[768,896]{1,0:T(8,128)}, u32[]{:S(2)}) %copy-start.4) | copy-done | bytes 2752536
  38.9 0.2 copy-done.11
  39.2 3.4 %fusion.19 = bf16[768,4,128]{0,2,1:T(8,128)(2,1)S(1)} fusion(bf16[768,4,128]{0,2,1:T(8,128)(2,1)S(1)} %bitcast.104, f32[768,4]{0,1:T(4,128)S(1)} %broadcast_minimum_fusion, f32[4,128]{1,0:T(4,128)S(1)} %concatenate.31, f32[768,896]{1,0:T(8,128)S(1)} %copy-done.4, f32[4]{0:T(128)S(1)} %copy-done.13, pred[4,896]{1,0:T(4,128)(4,1)S(1)} %broadcast_or_fusion, ...), kind=kOutput, calls=%fused_computation.29 | convolution fusion | flops 716701696 | bytes 5162512 | tf_op jit(solution)/shard_map/gij,jgc->igc/dot_general | solution.py:130
  42.6 2.2 %add_convert_fusion.1 = bf16[384,2048]{1,0:T(8,128)(2,1)} fusion(f32[384,2048]{1,0:T(8,128)S(1)} %fusion.39, bf16[512,2048]{1,0:T(8,128)(2,1)S(1)} %bitcast.92, bf16[768,512]{0,1:T(8,128)(2,1)S(1)} %bitcast.100, s32[]{:T(128)S(6)} %select_n.57), kind=kOutput, calls=%fused_computation.20 | convolution fusion | flops 806879232 | bytes 7208964 | tf_op jit(solution)/shard_map/dot_general | solution.py:152
  44.8 1.0 %fusion.42 = f32[384,2048]{1,0:T(8,128)S(1)} fusion(bf16[512,2048]{1,0:T(8,128)(2,1)S(1)} %bitcast.90, bf16[768,512]{0,1:T(8,128)(2,1)S(1)} %bitcast.96, s32[]{:T(128)S(6)} %select_n.52), kind=kOutput, calls=%fused_computation.56 | convolution fusion | flops 805306368 | bytes 5636100 | tf_op jit(solution)/shard_map/dot_general | solution.py:147
  45.8 2.7 %collective-permute-done.4 = bf16[384,2048]{1,0:T(8,128)(2,1)} collective-permute-done((bf16[384,2048]{1,0:T(8,128)(2,1)}, bf16[384,2048]{1,0:T(8,128)(2,1)}, u32[]{:S(2)}, u32[]{:S(2)}) %collective-permute-start.4) | collective-permute-done | bytes 1572896 | tf_op jit(solution)/shard_map/ppermute | solution.py:15
  48.5 3.7 %fusion.14 = bf16[1,384,2048]{2,1,0:T(8,128)(2,1)} fusion(bf16[384,2048]{1,0:T(8,128)(2,1)} %collective-permute-done.4, f32[384,2048]{1,0:T(8,128)S(1)} %fusion.42, bf16[512,2048]{1,0:T(8,128)(2,1)S(1)} %bitcast.93, bf16[768,512]{0,1:T(8,128)(2,1)S(1)} %bitcast.101, s32[]{:T(128)S(6)} %select_n.52), kind=kOutput, calls=%fused_computation.23 | convolution fusion | flops 808452096 | bytes 8781828 | tf_op jit(solution)/shard_map/dot_general | solution.py:152
  (65 shorter events, 1.3 us)
Async XLA Ops:
  0.0 37.0 %copy-start = (bf16[8,64,2048]{2,1,0:T(8,128)(2,1)S(1)}, bf16[8,64,2048]{2,1,0:T(8,128)(2,1)}, u32[]{:S(2)}) copy-start(bf16[8,64,2048]{2,1,0:T(8,128)(2,1)} %param.17) | copy-start | bytes 6291460
  0.0 5.9 %collective-permute-start = (bf16[768,1024]{1,0:T(8,128)(2,1)}, bf16[768,1024]{1,0:T(8,128)(2,1)}, u32[]{:S(2)}, u32[]{:S(2)}) collective-permute-start(bf16[768,1024]{1,0:T(8,128)(2,1)} %bitcast.97), channel_id=1, source_target_pairs={{0,1},{1,0},{2,3},{3,2},{4,5},{5,4},{6,7},{7,6},{8,9},{9,8},{10,11... | collective-permute-start | bytes 4718600 | tf_op jit(solution)/shard_map/ppermute | solution.py:15
  1.4 4.5 %copy-start.5 = (bf16[1,768,1024]{2,1,0:T(8,128)(2,1)S(1)}, bf16[1,768,1024]{2,1,0:T(8,128)(2,1)}, u32[]{:S(2)}) copy-start(bf16[1,768,1024]{2,1,0:T(8,128)(2,1)} %param.10) | copy-start | bytes 4718596
  7.5 0.7 %copy-start.12 = (f32[2048]{0:T(1024)S(1)}, f32[2048]{0:T(1024)}, u32[]{:S(2)}) copy-start(f32[2048]{0:T(1024)} %param.11) | copy-start | bytes 24580
  8.2 1.6 %copy-start.14 = (bf16[2048,4,128]{2,1,0:T(4,128)(2,1)S(1)}, bf16[2048,4,128]{2,1,0:T(4,128)(2,1)}, u32[]{:S(2)}) copy-start(bf16[2048,4,128]{2,1,0:T(4,128)(2,1)} %param.16) | copy-start | bytes 6291460
  9.3 6.4 %copy-start.3 = (bf16[768,2048]{1,0:T(8,128)(2,1)}, bf16[768,2048]{1,0:T(8,128)(2,1)S(1)}, u32[]{:S(2)}) copy-start(bf16[768,2048]{1,0:T(8,128)(2,1)S(1)} %fusion.6) | copy-start | bytes 9437188
  9.8 4.7 %copy-start.15 = (bf16[2048,2,64]{0,2,1:T(8,128)(2,1)S(1)}, bf16[2048,2,64]{0,2,1:T(8,128)(2,1)}, u32[]{:S(2)}) copy-start(bf16[2048,2,64]{0,2,1:T(8,128)(2,1)} %param.13) | copy-start | bytes 1572868
  11.7 4.1 %copy-start.10 = (bf16[768,512]{0,1:T(8,128)(2,1)}, bf16[768,512]{0,1:T(8,128)(2,1)S(1)}, u32[]{:S(2)}) copy-start(bf16[768,512]{0,1:T(8,128)(2,1)S(1)} %fusion.22) | copy-start | bytes 2359300
  11.7 4.1 %copy-start.16 = (bf16[2048,2,64]{0,2,1:T(8,128)(2,1)S(1)}, bf16[2048,2,64]{0,2,1:T(8,128)(2,1)}, u32[]{:S(2)}) copy-start(bf16[2048,2,64]{0,2,1:T(8,128)(2,1)} %param.14) | copy-start | bytes 1572868
  11.8 7.7 %collective-permute-start.2 = (f32[128]{0:T(128)S(1)}, f32[128]{0:T(128)S(1)}, u32[]{:S(2)}, u32[]{:S(2)}) collective-permute-start(f32[128]{0:T(128)S(1)} %convert_reduce_fusion), channel_id=1, source_target_pairs={{0,4},{4,8},{8,12},{12,0},{1,5},{5,9},{9,13},{13,1},{2,6},{6,10},{... | collective-permute-start | bytes 1544 | tf_op jit(solution)/shard_map/ppermute | solution.py:11
  17.9 12.0 %collective-permute-start.1 = (bf16[128,768]{0,1:T(8,128)(2,1)}, bf16[128,768]{0,1:T(8,128)(2,1)}, u32[]{:S(2)}, u32[]{:S(2)}) collective-permute-start(bf16[128,768]{0,1:T(8,128)(2,1)} %pad_maximum_fusion.3), channel_id=1, source_target_pairs={{0,4},{4,8},{8,12},{12,0},{1,5},{5,9},{9,13},{13,1},{2,6},{6,10},{... | collective-permute-start | bytes 589832 | tf_op jit(solution)/shard_map/ppermute | solution.py:11
  19.5 10.3 %collective-permute-start.3 = (f32[128]{0:T(128)S(1)}, f32[128]{0:T(128)S(1)}, u32[]{:S(2)}, u32[]{:S(2)}) collective-permute-start(f32[128]{0:T(128)S(1)} %fusion.55), channel_id=1, source_target_pairs={{0,8},{4,12},{8,0},{12,4},{1,9},{5,13},{9,1},{13,5},{2,10},{6,14},... | collective-permute-start | bytes 1544 | tf_op jit(solution)/shard_map/ppermute | solution.py:11
  29.9 2.7 %copy-start.8 = (bf16[128,768]{0,1:T(8,128)(2,1)}, bf16[128,768]{0,1:T(8,128)(2,1)S(1)}, u32[]{:S(2)}) copy-start(bf16[128,768]{0,1:T(8,128)(2,1)S(1)} %broadcast_select_fusion.2) | copy-start | bytes 589828
  37.0 1.8 %copy-start.4 = (f32[768,896]{1,0:T(8,128)S(1)}, f32[768,896]{1,0:T(8,128)}, u32[]{:S(2)}) copy-start(f32[768,896]{1,0:T(8,128)} %subtract_convert_fusion) | copy-start | bytes 8257540
  37.0 1.8 %slice-start = ((bf16[128,768]{0,1:T(8,128)(2,1)}), bf16[128,512]{0,1:T(8,128)(2,1)S(1)}, s32[]{:S(2)}) async-start(bf16[128,768]{0,1:T(8,128)(2,1)} %copy-done.8), calls=%async_computation | async-start | bytes 262144 | tf_op jit(solution)/shard_map/slice | solution.py:107
  37.0 1.9 %copy-start.9 = (pred[768,896]{1,0:T(8,128)(4,1)S(1)}, pred[768,896]{1,0:T(8,128)(4,1)}, u32[]{:S(2)}) copy-start(pred[768,896]{1,0:T(8,128)(4,1)} %broadcast_compare_fusion) | copy-start | bytes 2064388
  37.0 2.2 %copy-start.11 = (bf16[768,512]{0,1:T(8,128)(2,1)S(1)}, bf16[768,512]{0,1:T(8,128)(2,1)}, u32[]{:S(2)}) copy-start(bf16[768,512]{0,1:T(8,128)(2,1)} %copy-done.10) | copy-start | bytes 2359300
  37.0 2.2 %copy-start.13 = (f32[4]{0:T(128)S(1)}, f32[4]{0:T(128)}, u32[]{:S(2)}) copy-start(f32[4]{0:T(128)} %constant.17.clone) | copy-start | bytes 52
  39.2 3.4 %copy-start.1 = (bf16[4,128,2048]{2,1,0:T(8,128)(2,1)S(1)}, bf16[4,128,2048]{2,1,0:T(8,128)(2,1)}, u32[]{:S(2)}) copy-start(bf16[4,128,2048]{2,1,0:T(8,128)(2,1)} %param.18) | copy-start | bytes 6291460
  42.5 2.2 %copy-start.6 = (bf16[768,4,128]{0,2,1:T(8,128)(2,1)}, bf16[768,4,128]{0,2,1:T(8,128)(2,1)S(1)}, u32[]{:S(2)}) copy-start(bf16[768,4,128]{0,2,1:T(8,128)(2,1)S(1)} %fusion.19) | copy-start | bytes 2359300
  44.8 3.8 %collective-permute-start.4 = (bf16[384,2048]{1,0:T(8,128)(2,1)}, bf16[384,2048]{1,0:T(8,128)(2,1)}, u32[]{:S(2)}, u32[]{:S(2)}) collective-permute-start(bf16[384,2048]{1,0:T(8,128)(2,1)} %add_convert_fusion.1), channel_id=1, source_target_pairs={{0,1},{1,0},{2,3},{3,2},{4,5},{5,4},{6,7},{7,6},{8,9},{9,8},{10,11... | collective-permute-start | bytes 4718600 | tf_op jit(solution)/shard_map/ppermute | solution.py:15
  44.8 3.8 %copy-start.2 = (bf16[4,128,2048]{2,1,0:T(8,128)(2,1)S(1)}, bf16[4,128,2048]{2,1,0:T(8,128)(2,1)}, u32[]{:S(2)}) copy-start(bf16[4,128,2048]{2,1,0:T(8,128)(2,1)} %param.18) | copy-start | bytes 6291460
  44.8 3.8 %copy-start.7 = (bf16[768,4,128]{0,2,1:T(8,128)(2,1)S(1)}, bf16[768,4,128]{0,2,1:T(8,128)(2,1)}, u32[]{:S(2)}) copy-start(bf16[768,4,128]{0,2,1:T(8,128)(2,1)} %copy-done.6) | copy-start | bytes 2359300

commit v2 on v0

v2 whole, which is shorter than its diff:
```python
import functools

import jax
import jax.numpy as jnp
from jax import lax
from jax.experimental import pallas as pl
from jax.experimental.pallas import tpu as pltpu
from jax.sharding import PartitionSpec as P

WINDOW = 128
REACHES = (2, 4, 16)
BF16 = jnp.bfloat16
F32 = jnp.float32
VMEM = pl.BlockSpec(memory_space=pltpu.VMEM)
SMEM = pl.BlockSpec(memory_space=pltpu.SMEM)
ANY = pl.BlockSpec(memory_space=pl.ANY)


def from_behind(value, axis, steps):
    count = lax.axis_size(axis)
    return lax.ppermute(value, axis, [(i, (i + steps) % count) for i in range(count)])


def swap(value):
    return lax.ppermute(value, "tp", [(0, 1), (1, 0)])


def params(mib):
    return pltpu.CompilerParams(vmem_limit_bytes=mib * 2**20)


def dot(left, right, dims):
    return lax.dot_general(left, right, (dims, ((), ())), preferred_element_type=F32)


NN, NT, TN = ((1,), (0,)), ((1,), (1,)), ((0,), (0,))


def project_kernel(
    side_ref, gain_ref, mine, other, wq, wk, wv, wp,
    qkv_ref, pool_ref, tail_ref, total_ref,
    tokens, wqkv, wpool, normed, token_sem, weight_sem,
):
    rows, half = mine.shape
    queries, narrow, channels = wq.shape[0], wk.shape[0], wp.shape[1] // 4
    chunk = rows // 3 if rows % 3 == 0 else rows
    chunks = rows // chunk
    side = side_ref[0]
    token_copies = []
    for c in range(chunks):
        span = pl.ds(c * chunk, chunk)
        for i, source in enumerate((mine, other)):
            copy = pltpu.make_async_copy(
                source.at[span], tokens.at[i, span], token_sem.at[2 * c + i]
            )
            copy.start()
            token_copies.append(copy)
    weight_copies = [
        pltpu.make_async_copy(wq, wqkv.at[pl.ds(0, queries)], weight_sem.at[0]),
        pltpu.make_async_copy(wk, wqkv.at[pl.ds(queries, narrow)], weight_sem.at[1]),
        pltpu.make_async_copy(wv, wqkv.at[pl.ds(queries + narrow, narrow)], weight_sem.at[2]),
        pltpu.make_async_copy(wp, wpool, weight_sem.at[3]),
    ]
    for copy in weight_copies:
        copy.start()
    places = [pl.multiple_of(s * half, half) for s in (side, 1 - side)]
    gains = [gain_ref[:, pl.ds(place, half)] for place in places]
    block = 32

    def normalise(c):
        def body(i, _):
            span = pl.ds(pl.multiple_of(c * chunk + i * block, block), block)
            parts = [tokens[k, span, :].astype(F32) for k in range(2)]
            squares = sum(jnp.sum(part * part, axis=-1, keepdims=True) for part in parts)
            scale = lax.rsqrt(squares / (2 * half) + 1e-06)
            for part, gain, place in zip(parts, gains, places):
                normed[span, pl.ds(place, half)] = (part * scale * gain).astype(BF16)
            return 0

        lax.fori_loop(0, chunk // block, body, 0)

    for c in range(chunks):
        token_copies[2 * c].wait()
        token_copies[2 * c + 1].wait()
        normalise(c)
        if c == 0:
            for copy in weight_copies[:3]:
                copy.wait()
        span = pl.ds(c * chunk, chunk)
        qkv_ref[:, span] = dot(wqkv[...], normed[span, :], NT).astype(BF16)
    weight_copies[3].wait()
    step = 256
    for n in range(0, 4 * channels, step):
        pool_ref[:, n : n + step] = dot(normed[...], wpool[:, n : n + step], NN).astype(BF16)
    last = rows - WINDOW
    tail_ref[0 : 2 * narrow, :] = qkv_ref[queries:, last:]
    for g in range(3):
        at = 2 * narrow + 16 * g
        tail_ref[at : at + 16, :] = pool_ref[rows - 16 :, g * channels : (g + 1) * channels]
    total = jnp.sum(pool_ref[:, 3 * channels :].astype(F32), axis=0, keepdims=True)
    total_ref[...] = jnp.broadcast_to(total, total_ref.shape)


def project(side, gain, mine, other, wq, wk, wv, wp):
    rows, half = mine.shape
    width = 2 * half
    wide = wq.shape[0] + wk.shape[0] + wv.shape[0]
    channels = wp.shape[1] // 4
    chunks = 3 if rows % 3 == 0 else 1
    return pl.pallas_call(
        project_kernel,
        out_shape=(
            jax.ShapeDtypeStruct((wide, rows), BF16),
            jax.ShapeDtypeStruct((rows, 4 * channels), BF16),
            jax.ShapeDtypeStruct((2 * wk.shape[0] + 48, WINDOW), BF16),
            jax.ShapeDtypeStruct((8, channels), F32),
        ),
        in_specs=[SMEM, VMEM, ANY, ANY, ANY, ANY, ANY, ANY],
        out_specs=(VMEM,) * 4,
        scratch_shapes=[
            pltpu.VMEM((2, rows, half), BF16),
            pltpu.VMEM((wide, width), BF16),
            pltpu.VMEM((width, 4 * channels), BF16),
            pltpu.VMEM((rows, width), BF16),
            pltpu.SemaphoreType.DMA((2 * chunks,)),
            pltpu.SemaphoreType.DMA((4,)),
        ],
        compiler_params=params(32),
        cost_estimate=pl.CostEstimate(
            flops=2 * rows * width * (wide + 4 * channels),
            bytes_accessed=2 * (rows + wide + 4 * channels) * width,
            transcendentals=rows,
        ),
        name="project",
    )(side, gain, mine, other, wq, wk, wv, wp)


def attend_block(queries, keys, values, sinks_ref, valid):
    head_dim = 64
    heads = queries.shape[0] // head_dim
    local_kv = keys[0].shape[0] // head_dim
    group = heads // local_kv
    zero = jnp.zeros((head_dim, WINDOW), BF16)
    wide = jnp.concatenate(
        [
            jnp.concatenate(
                [
                    queries[h * head_dim : (h + 1) * head_dim] if h // group == v else zero
                    for h in range(heads)
                ],
                axis=1,
            )
            for v in range(local_kv)
        ],
        axis=0,
    )
    before = dot(keys[0], wide, TN)
    here = dot(keys[1], wide, TN)
    older = lax.broadcasted_iota(jnp.int32, (WINDOW, WINDOW), 0) > lax.broadcasted_iota(
        jnp.int32, (WINDOW, WINDOW), 1
    )
    outs = []
    for v in range(local_kv):
        olds, news = [], []
        for h in range(v * group, (v + 1) * group):
            lanes = slice(h * WINDOW, (h + 1) * WINDOW)
            past = before[:, lanes]
            if valid is not None:
                past = jnp.where(valid, past, -jnp.inf)
            score = jnp.where(older, past, here[:, lanes]) * head_dim ** (-0.5)
            sink = sinks_ref[h]
            top = jnp.maximum(jnp.max(score, axis=0, keepdims=True), sink)
            expo = jnp.exp(score - top)
            total = jnp.sum(expo, axis=0, keepdims=True) + jnp.exp(sink - top)
            weight = expo * (1.0 / total)
            olds.append(jnp.where(older, weight, 0.0).astype(BF16))
            news.append(jnp.where(older, 0.0, weight).astype(BF16))
        mine = slice(v * head_dim, (v + 1) * head_dim)
        out = dot(values[0][mine], jnp.concatenate(olds, axis=1), NN) + dot(
            values[1][mine], jnp.concatenate(news, axis=1), NN
        )
        outs += [out[:, g * WINDOW : (g + 1) * WINDOW] for g in range(group)]
    return jnp.concatenate(outs, axis=0).astype(BF16)


def attend_kernel(sinks_ref, qkv_ref, out_ref):
    wide, rows = qkv_ref.shape
    queries = out_ref.shape[0]
    narrow = (wide - queries) // 2

    def body(b, _):
        here = pl.ds(pl.multiple_of(b * WINDOW, WINDOW), WINDOW)
        past = pl.ds(pl.multiple_of((b - 1) * WINDOW, WINDOW), WINDOW)
        keys = [qkv_ref[queries : queries + narrow, s] for s in (past, here)]
        values = [qkv_ref[queries + narrow :, s] for s in (past, here)]
        out_ref[:, past] = attend_block(qkv_ref[:queries, here], keys, values, sinks_ref, None)
        return 0

    lax.fori_loop(1, rows // WINDOW, body, 0)


def attend(sinks, qkv, queries):
    wide, rows = qkv.shape
    return pl.pallas_call(
        attend_kernel,
        out_shape=jax.ShapeDtypeStruct((queries, rows - WINDOW), BF16),
        in_specs=[SMEM, VMEM],
        out_specs=VMEM,
        compiler_params=params(16),
        cost_estimate=pl.CostEstimate(
            flops=3 * 10**9, bytes_accessed=2 * wide * rows, transcendentals=rows * 1024
        ),
        name="attend",
    )(sinks, qkv)


def finish_kernel(sinks_ref, place_ref, qkv_ref, pool_ref, tail_ref, carry_ref, out_ref, pooled_ref, ext):
    wide, rows = qkv_ref.shape
    queries = out_ref.shape[0]
    narrow = (wide - queries) // 2
    channels = pool_ref.shape[1] // 4
    place = place_ref[0]
    here = slice(0, WINDOW)
    keys = [tail_ref[:narrow, :], qkv_ref[queries : queries + narrow, here]]
    values = [tail_ref[narrow : 2 * narrow, :], qkv_ref[queries + narrow :, here]]
    out_ref[...] = attend_block(qkv_ref[:queries, here], keys, values, sinks_ref, place > 0)

    count = (
        lax.broadcasted_iota(jnp.int32, (rows, channels), 0) + (place * rows + 1)
    ).astype(F32)
    for g, reach in enumerate(REACHES):
        lanes = slice(g * channels, (g + 1) * channels)
        at = 2 * narrow + 16 * g
        ext[0:16, :] = jnp.zeros((16, channels), F32)
        ext[16:32, :] = jnp.where(place > 0, tail_ref[at : at + 16, :].astype(F32), 0.0)
        ext[32:, :] = pool_ref[:, lanes].astype(F32)
        low = 1
        while low < reach:
            ext[8:, :] = ext[8:, :] + ext[8 - low : 32 + rows - low, :]
            low *= 2
        summed = ext[32:, :]
        own = pool_ref[:, lanes].astype(F32)
        mean = summed / jnp.minimum(count, float(reach))
        pooled_ref[:, lanes] = (mean - own).astype(BF16)
    lanes = slice(3 * channels, 4 * channels)
    blocks = rows // WINDOW
    lower = (
        lax.broadcasted_iota(jnp.int32, (WINDOW, WINDOW), 0)
        >= lax.broadcasted_iota(jnp.int32, (WINDOW, WINDOW), 1)
    ).astype(BF16)
    side_by_side = jnp.concatenate(
        [pool_ref[b * WINDOW : (b + 1) * WINDOW, lanes] for b in range(blocks)], axis=1
    )
    sums = dot(lower, side_by_side, NN)
    running = carry_ref[0:1, :]
    for b in range(blocks):
        span = slice(b * WINDOW, (b + 1) * WINDOW)
        inner = sums[:, b * channels : (b + 1) * channels]
        mean = (inner + running) / count[span]
        pooled_ref[span, lanes] = (mean - pool_ref[span, lanes].astype(F32)).astype(BF16)
        running = running + inner[WINDOW - 1 :, :]


def finish(sinks, place, qkv, pool, tail, carry, queries):
    wide, rows = qkv.shape
    channels = pool.shape[1] // 4
    return pl.pallas_call(
        finish_kernel,
        out_shape=(
            jax.ShapeDtypeStruct((queries, WINDOW), BF16),
            jax.ShapeDtypeStruct(pool.shape, BF16),
        ),
        in_specs=[SMEM, SMEM, VMEM, VMEM, VMEM, VMEM],
        out_specs=(VMEM, VMEM),
        scratch_shapes=[pltpu.VMEM((rows + 32, channels), F32)],
        compiler_params=params(24),
        cost_estimate=pl.CostEstimate(
            flops=10**9, bytes_accessed=2 * wide * rows, transcendentals=1024 * 128
        ),
        name="finish",
    )(sinks, place, qkv, pool, tail, carry)


def shards(
    tokens,
    norm_gain,
    query_weight,
    key_weight,
    value_weight,
    sink_logit,
    pool_weight,
    attn_out_weight,
    pool_out_weight,
):
    mine = tokens[0]
    other = swap(mine)
    rows = mine.shape[0]
    width = norm_gain.shape[0]
    side = lax.axis_index("tp")
    place = lax.axis_index("sp")

    def rows_of(weight):
        return weight.transpose(1, 2, 0).reshape(-1, width)

    qkv, pool, tail, total = project(
        side[None],
        norm_gain[None],
        mine,
        other,
        rows_of(query_weight),
        rows_of(key_weight),
        rows_of(value_weight),
        pool_weight.reshape(width, -1),
    )
    queries = query_weight.shape[1] * query_weight.shape[2]
    tail = from_behind(tail, "sp", 1)
    count = lax.axis_size("sp")
    carried = jnp.zeros_like(total)
    if count <= 4:
        for steps in range(1, count):
            got = from_behind(total, "sp", steps)
            carried = carried + jnp.where(place >= steps, got, 0.0)
    else:
        running = total
        steps = 1
        while steps < count:
            got = jnp.where(place >= steps, from_behind(running, "sp", steps), 0.0)
            carried = carried + got
            running = running + got
            steps *= 2
    later = attend(sink_logit, qkv, queries)
    first, pooled = finish(sink_logit, place[None], qkv, pool, tail, carried, queries)
    attended = jnp.concatenate([first, later], axis=1)
    attn_rows = attn_out_weight.reshape(-1, width)
    pool_weight_rows = pool_out_weight.reshape(-1, width)
    half = rows // 2

    def merge(start):
        part = dot(lax.dynamic_slice_in_dim(attended, start, half, 1), attn_rows, TN)
        return part + dot(lax.dynamic_slice_in_dim(pooled, start, half, 0), pool_weight_rows, NN)

    given = swap(merge((1 - side) * half).astype(BF16))
    result = (merge(side * half) + given.astype(F32)).astype(BF16)
    return result[None]


def solution(mesh):
    in_specs = (
        P("fs", ("grp", "sp"), "tp"),
        P(),
        P(None, "tp", None),
        P(None, "tp", None),
        P(None, "tp", None),
        P("tp"),
        P(None, None, "tp"),
        P("tp", None, None),
        P(None, "tp", None),
    )
    out_specs = P("fs", ("grp", "sp", "tp"), None)
    return jax.shard_map(shards, mesh=mesh, in_specs=in_specs, out_specs=out_specs, check_vma=False)
```

time: 104 us -> 44.7 us (0.43)
  matrix products: 30.6 us -> 6.31 us
  waiting for transfers between devices: 20.8 us -> 0.64 us
  Pallas kernels: 0 us -> 16.3 us
  between operations: 13.7 us -> 0.15 us
  other arithmetic: 12 us -> 3.47 us
  blocking collectives: 8.46 us -> 0 us
  starting transfers between devices: 11.4 us -> 8.94 us
  local copies, waits for them, and re-layouts: 6.9 us -> 8.61 us
    dot_general x8 -> x4, matrix products: 30.6 us -> 6.31 us  [dot(): lax.dot_general(left, right, (dims, ((), ())), preferred_element_type=F32)]
    pallas_call x0 -> x3, Pallas kernels: none -> 16.3 us  [the longest x1 10.8 us: project(): pl.pallas_call(project_kernel, out_shape=(jax.ShapeDtypeStruct((wide, row...]
    all_gather x1 -> x0, waiting for transfers between devices: 10.6 us -> none  [shards(): whole = lax.all_gather(tokens, 'tp', axis=2, tiled=True)[0]]
    reduce_scatter x1 -> x0, waiting for transfers between devices: 9.46 us -> none  [shards(): lax.psum_scatter((part_sum + jnp.dot(pooled, pool_weight_rows, preferred_...]
    unnamed x22 -> x23, local copies, waits for them, and re-layouts: 0.14 us -> 8.61 us
    all_gather x1 -> x0, blocking collectives: 8.46 us -> none  [shards(): totals = lax.all_gather(prefix_total[None], 'sp', axis=0, tiled=True)]
    reduce_sum x4 -> x0, other arithmetic: 5.18 us -> none  [the longest x1 2.72 us: rms_norm(): scale = lax.rsqrt(jnp.mean(values * values, axis=-1, keepdims=True) + 1e-06)]
    reshape x5 -> x0, local copies, waits for them, and re-layouts: 4.17 us -> none  [the longest x1 3.63 us: attend(): qb = query.reshape(blocks, WINDOW, local_kv, group, head_dim)]
  transfers between devices with their start and end apart: 5 -> 6, of which waited for: 2 -> 1; matrix products, arithmetic and copies ran while one was open for 28% -> 15% of each run, Pallas kernels for 0% -> 8%
where the time goes in v2:
time: 44.7 us; the launch traced here: 44.4 us
  Pallas kernels  16.3 us (36%)
  starting transfers between devices  8.94 us (20%)
  local copies, waits for them, and re-layouts  8.61 us (19%)
  matrix products  6.31 us (14%)
  other arithmetic  3.47 us (8%)
  waiting for transfers between devices  0.64 us (1%)
    pallas_call x1, Pallas kernels, project(): pl.pallas_call(project_kernel, out_shape=(jax.ShapeDtypeStruct((wide, row...  10.8 us
    unnamed x23, local copies, waits for them, and re-layouts  8.61 us
    ppermute x4, starting transfers between devices, from_behind(): lax.ppermute(value, axis, [(i, (i + steps) % count) for i in range(count)])  8.44 us
    dot_general x4, matrix products, dot(): lax.dot_general(left, right, (dims, ((), ())), preferred_element_type=F32)  6.31 us
    pallas_call x1, Pallas kernels, attend(): pl.pallas_call(attend_kernel, out_shape=jax.ShapeDtypeStruct((queries, ro...  3.7 us
    broadcast_in_dim x1, other arithmetic, shards(): return result[None]  3.46 us
    pallas_call x1, Pallas kernels, finish(): pl.pallas_call(finish_kernel, out_shape=(jax.ShapeDtypeStruct((queries, W...  1.76 us
  transfers between devices with their start and end apart: 6, of which 1 were waited for; matrix products, arithmetic and copies ran while one was open for 15% of the time, Pallas kernels for 8%

profile of v2, /device:TPU:0, one launch (start us, length us, event | category | flops | bytes accessed | tf_op | source)
XLA Modules:
  0.0 44.4 jit_solution(8895714476767384820)
XLA Ops:
  0.0 0.0 copy-start
  0.0 0.5 %collective-permute-start = (bf16[768,1024]{1,0:T(8,128)(2,1)}, bf16[768,1024]{1,0:T(8,128)(2,1)}, u32[]{:S(2)}, u32[]{:S(2)}) collective-permute-start(bf16[768,1024]{1,0:T(8,128)(2,1)} %bitcast.29), channel_id=1, source_target_pairs={{0,1},{1,0},{2,3},{3,2},{4,5},{5,4},{6,7},{7,6},{8,9},{9,8},{10,11... | collective-permute-start | bytes 4718600 | tf_op jit(solution)/shard_map/ppermute | solution.py:25
  0.5 3.4 %copy.12 = bf16[256,8,4,128]{3,1,2,0:T(8,128)(2,1)} copy(bf16[256,8,4,128]{3,2,1,0:T(4,128)(2,1)} %bitcast.36) | data formatting | bytes 4194304
  3.9 0.0 collective-permute-done.other
  3.9 0.0 copy-done.5
  3.9 0.0 copy-done.6
  3.9 0.0 copy-done.7
  3.9 0.0 copy-start.1
  4.0 1.6 %copy-done.1 = bf16[256,8,4,128]{3,1,2,0:T(8,128)(2,1)S(1)} copy-done((bf16[256,8,4,128]{3,1,2,0:T(8,128)(2,1)S(1)}, bf16[256,8,4,128]{3,1,2,0:T(8,128)(2,1)}, u32[]{:S(2)}) %copy-start.1) | copy-done | bytes 2097176
  5.5 1.6 %copy-done.3 = bf16[2048,8,64]{0,2,1:T(8,128)(2,1)S(1)} copy-done((bf16[2048,8,64]{0,2,1:T(8,128)(2,1)S(1)}, bf16[2048,8,64]{0,2,1:T(8,128)(2,1)}, u32[]{:S(2)}) %copy-start.3) | copy-done | bytes 2097176
  7.1 1.4 %copy-done.4 = bf16[1,768,1024]{2,1,0:T(8,128)(2,1)S(1)} copy-done((bf16[1,768,1024]{2,1,0:T(8,128)(2,1)S(1)}, bf16[1,768,1024]{2,1,0:T(8,128)(2,1)}, u32[]{:S(2)}) %copy-start.4) | copy-done | bytes 1572888
  8.5 10.8 %project.1 = (bf16[768,768]{1,0:T(8,128)(2,1)S(1)}, bf16[768,512]{1,0:T(8,128)(2,1)S(1)}, bf16[304,128]{1,0:T(8,128)(2,1)S(1)}, f32[8,128]{1,0:T(8,128)S(1)}) custom-call(s32[1]{0:T(128)} %bitcast.1.side_ref, f32[1,2048]{1,0:T(1,128)S(1)} %bitcast.33, bf16[768,1024]{1,0:T(8,128)(2,1)S(1)} %bitcast.30, bf16[768,1024]{1,0:T(8,128)(2,1)} %collective-permute-done.other, ...), custom_call_target="tpu_custom_call" | custom-call | flops 4026531840 | bytes 8388608 | tf_op jit(solution)/shard_map/project/pallas_call | solution.py:110
  19.4 5.0 %collective-permute-start.4 = (f32[8,128]{1,0:T(8,128)S(1)}, f32[8,128]{1,0:T(8,128)S(1)}, u32[]{:S(2)}, u32[]{:S(2)}) collective-permute-start(f32[8,128]{1,0:T(8,128)S(1)} %get-tuple-element.14), channel_id=1, source_target_pairs={{0,12},{4,0},{8,4},{12,8},{1,13},{5,1},{9,5},{13,9},{2,14},{6,2},{... | collective-permute-start | bytes 12296 | tf_op jit(solution)/shard_map/ppermute | solution.py:21
  24.3 0.0 collective-permute-start.3
  24.3 1.0 %collective-permute-start.2 = (f32[8,128]{1,0:T(8,128)S(1)}, f32[8,128]{1,0:T(8,128)S(1)}, u32[]{:S(2)}, u32[]{:S(2)}) collective-permute-start(f32[8,128]{1,0:T(8,128)S(1)} %get-tuple-element.14), channel_id=1, source_target_pairs={{0,4},{4,8},{8,12},{12,0},{1,5},{5,9},{9,13},{13,1},{2,6},{6,10},{... | collective-permute-start | bytes 12296 | tf_op jit(solution)/shard_map/ppermute | solution.py:21
  25.3 2.5 %collective-permute-start.1 = (bf16[304,128]{1,0:T(8,128)(2,1)S(1)}, bf16[304,128]{1,0:T(8,128)(2,1)S(1)}, u32[]{:S(2)}, u32[]{:S(2)}) collective-permute-start(bf16[304,128]{1,0:T(8,128)(2,1)S(1)} %get-tuple-element.13), channel_id=1, source_target_pairs={{0,4},{4,8},{8,12},{12,0},{1,5},{5,9},{9,13},{13,1},{2,6},{6,10},{... | collective-permute-start | bytes 233480 | tf_op jit(solution)/shard_map/ppermute | solution.py:21
  27.8 0.0 copy-done.8
  27.8 3.7 %attend.1 = bf16[512,640]{1,0:T(8,128)(2,1)S(1)} custom-call(f32[8]{0:T(128)S(1)} %copy-done.8, bf16[768,768]{1,0:T(8,128)(2,1)S(1)} %get-tuple-element.11.qkv_ref), custom_call_target="tpu_custom_call" | custom-call | flops 3000000000 | bytes 1179648 | tf_op jit(solution)/shard_map/attend/pallas_call | solution.py:204
  31.5 0.0 collective-permute-done.4
  31.5 0.0 collective-permute-done.3
  31.5 0.0 collective-permute-done.2
  31.6 0.0 collective-permute-done.1.tail_ref
  31.6 1.8 %finish.1 = (bf16[512,128]{1,0:T(8,128)(2,1)S(1)}, bf16[768,512]{1,0:T(8,128)(2,1)S(1)}) custom-call(f32[8]{0:T(128)S(1)} %copy-done.8, s32[1]{0:T(128)} %bitcast.place_ref, bf16[768,768]{1,0:T(8,128)(2,1)S(1)} %get-tuple-element.11.qkv_ref, bf16[768,512]{1,0:T(8,128)(2,1)S(1)} %get-tuple-element.12.pool_ref, ...), custom_call_target="tpu_custom_call" | custom-call | flops 1000000000 | bytes 1179648 | tf_op jit(solution)/shard_map/finish/pallas_call | solution.py:267
  33.3 0.0 copy-start.9
  33.4 1.0 %fusion.2 = f32[384,2048]{1,0:T(8,128)S(1)} fusion(bf16[512,2048]{1,0:T(8,128)(2,1)S(1)} %bitcast.26, s32[]{:T(128)S(6)} %select_n.35, bf16[512,640]{1,0:T(8,128)(2,1)S(1)} %attend.1, bf16[512,128]{1,0:T(8,128)(2,1)S(1)} %get-tuple-element.15), kind=kOutput, calls=%fused_computation.9 | convolution fusion | flops 806092800 | bytes 6029316 | tf_op jit(solution)/shard_map/dot_general | solution.py:33
  34.4 0.6 %copy-done.9 = bf16[4,128,2048]{2,1,0:T(8,128)(2,1)S(1)} copy-done((bf16[4,128,2048]{2,1,0:T(8,128)(2,1)S(1)}, bf16[4,128,2048]{2,1,0:T(8,128)(2,1)}, u32[]{:S(2)}) %copy-start.9) | copy-done | bytes 2097176
  35.0 2.2 %add_convert_fusion.1 = bf16[384,2048]{1,0:T(8,128)(2,1)} fusion(f32[384,2048]{1,0:T(8,128)S(1)} %fusion.2, bf16[512,2048]{1,0:T(8,128)(2,1)S(1)} %bitcast.34, bf16[768,512]{1,0:T(8,128)(2,1)S(1)} %get-tuple-element.16, s32[]{:T(128)S(6)} %select_n.35), kind=kOutput, calls=%fused_computation.1 | convolution fusion | flops 806879232 | bytes 7208964 | tf_op jit(solution)/shard_map/dot_general | solution.py:33
  37.2 0.0 collective-permute-start.5
  37.2 2.1 %fusion.5 = f32[384,2048]{1,0:T(8,128)S(1)} fusion(bf16[512,2048]{1,0:T(8,128)(2,1)S(1)} %bitcast.25, s32[]{:T(128)S(6)} %select_n.34, bf16[512,640]{1,0:T(8,128)(2,1)S(1)} %attend.1, bf16[512,128]{1,0:T(8,128)(2,1)} %copy-done.2), kind=kOutput, calls=%fused_computation.11 | convolution fusion | flops 806092800 | bytes 6029316 | tf_op jit(solution)/shard_map/dot_general | solution.py:33
  39.3 1.0 %fusion.8 = f32[384,2048]{1,0:T(8,128)S(1)} fusion(bf16[512,2048]{1,0:T(8,128)(2,1)S(1)} %bitcast.35, bf16[768,512]{1,0:T(8,128)(2,1)S(1)} %get-tuple-element.16, s32[]{:T(128)S(6)} %select_n.34), kind=kOutput, calls=%fused_computation.13 | convolution fusion | flops 805306368 | bytes 5636100 | tf_op jit(solution)/shard_map/dot_general | solution.py:33
  40.3 0.6 %collective-permute-done.5 = bf16[384,2048]{1,0:T(8,128)(2,1)} collective-permute-done((bf16[384,2048]{1,0:T(8,128)(2,1)}, bf16[384,2048]{1,0:T(8,128)(2,1)}, u32[]{:S(2)}, u32[]{:S(2)}) %collective-permute-start.5) | collective-permute-done | bytes 1572896 | tf_op jit(solution)/shard_map/ppermute | solution.py:25
  40.9 3.5 %fusion = bf16[1,384,2048]{2,1,0:T(8,128)(2,1)} fusion(bf16[384,2048]{1,0:T(8,128)(2,1)} %collective-permute-done.5, f32[384,2048]{1,0:T(8,128)S(1)} %fusion.5, f32[384,2048]{1,0:T(8,128)S(1)} %fusion.8), kind=kLoop, calls=%fused_computation.3 | loop fusion | flops 3145728 | bytes 9437184 | tf_op jit(solution)/shard_map/broadcast_in_dim | solution.py:344
  (12 shorter events, 0.0 us)
Async XLA Ops:
  0.0 33.3 %copy-start = (bf16[8,64,2048]{2,1,0:T(8,128)(2,1)S(1)}, bf16[8,64,2048]{2,1,0:T(8,128)(2,1)}, u32[]{:S(2)}) copy-start(bf16[8,64,2048]{2,1,0:T(8,128)(2,1)} %param.16) | copy-start | bytes 6291460
  0.0 3.9 %collective-permute-start = (bf16[768,1024]{1,0:T(8,128)(2,1)}, bf16[768,1024]{1,0:T(8,128)(2,1)}, u32[]{:S(2)}, u32[]{:S(2)}) collective-permute-start(bf16[768,1024]{1,0:T(8,128)(2,1)} %bitcast.29), channel_id=1, source_target_pairs={{0,1},{1,0},{2,3},{3,2},{4,5},{5,4},{6,7},{7,6},{8,9},{9,8},{10,11... | collective-permute-start | bytes 4718600 | tf_op jit(solution)/shard_map/ppermute | solution.py:25
  0.5 3.4 %copy-start.5 = (bf16[2048,2,64]{0,2,1:T(8,128)(2,1)S(1)}, bf16[2048,2,64]{0,2,1:T(8,128)(2,1)}, u32[]{:S(2)}) copy-start(bf16[2048,2,64]{0,2,1:T(8,128)(2,1)} %param.12) | copy-start | bytes 1572868
  0.5 3.4 %copy-start.6 = (bf16[2048,2,64]{0,2,1:T(8,128)(2,1)S(1)}, bf16[2048,2,64]{0,2,1:T(8,128)(2,1)}, u32[]{:S(2)}) copy-start(bf16[2048,2,64]{0,2,1:T(8,128)(2,1)} %param.13) | copy-start | bytes 1572868
  0.5 3.4 %copy-start.7 = (f32[2048]{0:T(1024)S(1)}, f32[2048]{0:T(1024)}, u32[]{:S(2)}) copy-start(f32[2048]{0:T(1024)} %param.10) | copy-start | bytes 24580
  3.9 1.6 %copy-start.1 = (bf16[256,8,4,128]{3,1,2,0:T(8,128)(2,1)S(1)}, bf16[256,8,4,128]{3,1,2,0:T(8,128)(2,1)}, u32[]{:S(2)}) copy-start(bf16[256,8,4,128]{3,1,2,0:T(8,128)(2,1)} %copy.12) | copy-start | bytes 6291460
  5.5 1.6 %copy-start.3 = (bf16[2048,8,64]{0,2,1:T(8,128)(2,1)S(1)}, bf16[2048,8,64]{0,2,1:T(8,128)(2,1)}, u32[]{:S(2)}) copy-start(bf16[2048,8,64]{0,2,1:T(8,128)(2,1)} %param.11) | copy-start | bytes 6291460
  7.1 1.4 %copy-start.4 = (bf16[1,768,1024]{2,1,0:T(8,128)(2,1)S(1)}, bf16[1,768,1024]{2,1,0:T(8,128)(2,1)}, u32[]{:S(2)}) copy-start(bf16[1,768,1024]{2,1,0:T(8,128)(2,1)} %param.9) | copy-start | bytes 4718596
  8.5 19.3 %copy-start.8 = (f32[8]{0:T(128)S(1)}, f32[8]{0:T(128)}, u32[]{:S(2)}) copy-start(f32[8]{0:T(128)} %sinks_ref.3) | copy-start | bytes 100
  19.4 12.2 %collective-permute-start.4 = (f32[8,128]{1,0:T(8,128)S(1)}, f32[8,128]{1,0:T(8,128)S(1)}, u32[]{:S(2)}, u32[]{:S(2)}) collective-permute-start(f32[8,128]{1,0:T(8,128)S(1)} %get-tuple-element.14), channel_id=1, source_target_pairs={{0,12},{4,0},{8,4},{12,8},{1,13},{5,1},{9,5},{13,9},{2,14},{6,2},{... | collective-permute-start | bytes 12296 | tf_op jit(solution)/shard_map/ppermute | solution.py:21
  24.3 7.2 %collective-permute-start.3 = (f32[8,128]{1,0:T(8,128)S(1)}, f32[8,128]{1,0:T(8,128)S(1)}, u32[]{:S(2)}, u32[]{:S(2)}) collective-permute-start(f32[8,128]{1,0:T(8,128)S(1)} %get-tuple-element.14), channel_id=1, source_target_pairs={{0,8},{4,12},{8,0},{12,4},{1,9},{5,13},{9,1},{13,5},{2,10},{6,14},... | collective-permute-start | bytes 12296 | tf_op jit(solution)/shard_map/ppermute | solution.py:21
  24.3 7.2 %collective-permute-start.2 = (f32[8,128]{1,0:T(8,128)S(1)}, f32[8,128]{1,0:T(8,128)S(1)}, u32[]{:S(2)}, u32[]{:S(2)}) collective-permute-start(f32[8,128]{1,0:T(8,128)S(1)} %get-tuple-element.14), channel_id=1, source_target_pairs={{0,4},{4,8},{8,12},{12,0},{1,5},{5,9},{9,13},{13,1},{2,6},{6,10},{... | collective-permute-start | bytes 12296 | tf_op jit(solution)/shard_map/ppermute | solution.py:21
  25.3 6.2 %collective-permute-start.1 = (bf16[304,128]{1,0:T(8,128)(2,1)S(1)}, bf16[304,128]{1,0:T(8,128)(2,1)S(1)}, u32[]{:S(2)}, u32[]{:S(2)}) collective-permute-start(bf16[304,128]{1,0:T(8,128)(2,1)S(1)} %get-tuple-element.13), channel_id=1, source_target_pairs={{0,4},{4,8},{8,12},{12,0},{1,5},{5,9},{9,13},{13,1},{2,6},{6,10},{... | collective-permute-start | bytes 233480 | tf_op jit(solution)/shard_map/ppermute | solution.py:21
  33.3 1.1 %copy-start.2 = (bf16[512,128]{1,0:T(8,128)(2,1)}, bf16[512,128]{1,0:T(8,128)(2,1)S(1)}, u32[]{:S(2)}) copy-start(bf16[512,128]{1,0:T(8,128)(2,1)S(1)} %get-tuple-element.15) | copy-start | bytes 393220
  33.3 1.6 %copy-start.9 = (bf16[4,128,2048]{2,1,0:T(8,128)(2,1)S(1)}, bf16[4,128,2048]{2,1,0:T(8,128)(2,1)}, u32[]{:S(2)}) copy-start(bf16[4,128,2048]{2,1,0:T(8,128)(2,1)} %param.17) | copy-start | bytes 6291460
  37.2 3.8 %collective-permute-start.5 = (bf16[384,2048]{1,0:T(8,128)(2,1)}, bf16[384,2048]{1,0:T(8,128)(2,1)}, u32[]{:S(2)}, u32[]{:S(2)}) collective-permute-start(bf16[384,2048]{1,0:T(8,128)(2,1)} %add_convert_fusion.1), channel_id=1, source_target_pairs={{0,1},{1,0},{2,3},{3,2},{4,5},{5,4},{6,7},{7,6},{8,9},{9,8},{10,11... | collective-permute-start | bytes 4718600 | tf_op jit(solution)/shard_map/ppermute | solution.py:25
  37.2 2.1 %copy-start.10 = (bf16[4,128,2048]{2,1,0:T(8,128)(2,1)S(1)}, bf16[4,128,2048]{2,1,0:T(8,128)(2,1)}, u32[]{:S(2)}) copy-start(bf16[4,128,2048]{2,1,0:T(8,128)(2,1)} %param.17) | copy-start | bytes 6291460
